TPU v7x, 32 devices: a whole 2x2x4 slice. The times are simulated.
32 devices in a mesh: rep: 2 (over y), fs: 4 (over z), tp: 4 (over x, core).
Axes of the slice: x: 2, y: 2, z: 4, core: 2. Of those that a mesh axis runs over, the one named last changes fastest.
Arguments:
- stream: bfloat16 [4096, 2048], P(('rep', 'fs', 'tp')), may hold values from -6 to 6
- gain_before: float32 [2048], replicated, may hold values from 0.1 to 1.9
- gain_after: float32 [2048], replicated, may hold values from 0.1 to 1.9
- proj_gate: bfloat16 [2048, 3584], P('fs', 'tp'), may hold values from -0.125 to 0.125
- proj_lift: bfloat16 [2048, 3584], P('fs', 'tp'), may hold values from -0.125 to 0.125
- proj_down: bfloat16 [3584, 2048], P('tp', 'fs'), may hold values from -0.09375 to 0.09375
- mixer_gain: float32 [2048], replicated, may hold values from 0.1 to 1.9
- mixer_u: bfloat16 [2048, 2048], P('fs', 'tp'), may hold values from -0.125 to 0.125
- mixer_v: bfloat16 [2048, 2048], P('fs', 'tp'), may hold values from -1 to 1
- layer_gain: float32 [2048], P('tp'), may hold values from 0.1 to 1.9
- layer_shift: float32 [2048], P('tp'), may hold values from -3 to 3
- spatial: bfloat16 [16, 128, 128], P('tp'), may hold values from -0.5 to 0.5
- spatial_shift: float32 [16, 128], P('tp'), may hold values from 0.2 to 2
- mixer_down: bfloat16 [2048, 2048], P('tp', 'fs'), may hold values from -0.125 to 0.125
Outputs:
- result: bfloat16 [4096, 2048], P(('rep', 'fs', 'tp'))
All inputs are finite; a program needn't handle non-finite values.
Results may differ from a plain program's by a relative error of at most 0.017.
Values may be sent and summed in bfloat16 or wider, within the bound.
A program may use at most 128 MiB of HBM per device.

v0:
```python
import jax
import jax.numpy as jnp
from jax import lax
from jax.sharding import PartitionSpec as P

GROUP_DIM = 128
SPAN = 128
A = 2048


norm_epsilon = 1e-06
layer_epsilon = 1e-05


def norm_rows(row_block, scale_gain):
    widened = row_block.astype(jnp.float32)
    factor = lax.rsqrt(jnp.mean(widened * widened, axis=1, keepdims=True) + norm_epsilon)
    return (widened * factor * scale_gain).astype(jnp.bfloat16)


def gathered_norm(stream_rows, scale_gain):
    gathered = lax.all_gather(stream_rows, "tp", axis=0, tiled=True)
    return norm_rows(gathered, scale_gain)


def pair_adder(normed, pieces):
    return (
        jnp.dot(normed, pieces[0], preferred_element_type=jnp.float32),
        jnp.dot(normed, pieces[1], preferred_element_type=jnp.float32),
    )


def activate(gate_vals, lift_vals):
    return (jax.nn.silu(gate_vals) * lift_vals).astype(jnp.bfloat16)


def half_again(stream_rows, scale_gain, proj_gate, proj_lift, proj_down):
    normed = gathered_norm(stream_rows, scale_gain)
    gate_vals, lift_vals = pair_adder(
        normed,
        (
            lax.all_gather(proj_gate, "fs", axis=0, tiled=True),
            lax.all_gather(proj_lift, "fs", axis=0, tiled=True),
        ),
    )
    hidden = activate(gate_vals, lift_vals)
    partial_value = jnp.dot(
        hidden,
        lax.all_gather(proj_down, "fs", axis=1, tiled=True),
        preferred_element_type=jnp.float32,
    )
    summed = lax.psum_scatter(
        partial_value.astype(jnp.bfloat16), "tp", scatter_dimension=0, tiled=True
    ).astype(jnp.float32)
    return (stream_rows.astype(jnp.float32) + 0.5 * summed).astype(jnp.bfloat16)


def token_mixer(
    stream_rows,
    mixer_gain,
    mixer_u,
    mixer_v,
    layer_gain,
    layer_shift,
    spatial,
    spatial_shift,
    mixer_down,
):
    gathered = lax.all_gather(stream_rows, "tp", axis=0, tiled=True)
    normed = norm_rows(gathered, mixer_gain)
    seq_tokens = normed.shape[0]
    u_vals, v_vals = pair_adder(
        normed,
        (
            lax.all_gather(mixer_u, "fs", axis=0, tiled=True),
            lax.all_gather(mixer_v, "fs", axis=0, tiled=True),
        ),
    )
    lifted = jax.nn.gelu(v_vals)
    moments = lax.psum((jnp.sum(lifted, axis=1), jnp.sum(lifted * lifted, axis=1)), "tp")
    centre = moments[0] / A
    spread = moments[1] / A - centre * centre
    normed_v = (
        (lifted - centre[:, None]) * lax.rsqrt(spread[:, None] + layer_epsilon) * layer_gain
        + layer_shift
    ).astype(jnp.bfloat16)
    groups_here = spatial.shape[0]
    blocked = normed_v.reshape(seq_tokens // SPAN, SPAN, groups_here, GROUP_DIM)
    causal = jnp.tril(jnp.ones((SPAN, SPAN), dtype=bool))
    masked = jnp.where(causal[None], spatial, jnp.zeros((), jnp.bfloat16))
    mixed_v = jnp.einsum("gts,bsgd->btgd", masked, blocked, preferred_element_type=jnp.float32)
    mixed_v = mixed_v + spatial_shift.T[None, :, :, None]
    gated = (jax.nn.gelu(u_vals) * mixed_v.reshape(seq_tokens, groups_here * GROUP_DIM)).astype(
        jnp.bfloat16
    )
    partial_value = jnp.dot(
        gated,
        lax.all_gather(mixer_down, "fs", axis=1, tiled=True),
        preferred_element_type=jnp.float32,
    )
    summed = lax.psum_scatter(
        partial_value.astype(jnp.bfloat16), "tp", scatter_dimension=0, tiled=True
    ).astype(jnp.float32)
    return (stream_rows.astype(jnp.float32) + summed).astype(jnp.bfloat16)


def body(
    stream,
    gain_before,
    gain_after,
    proj_gate,
    proj_lift,
    proj_down,
    mixer_gain,
    mixer_u,
    mixer_v,
    layer_gain,
    layer_shift,
    spatial,
    spatial_shift,
    mixer_down,
):
    first = half_again(stream, gain_before, proj_gate, proj_lift, proj_down)
    second = token_mixer(
        first,
        mixer_gain,
        mixer_u,
        mixer_v,
        layer_gain,
        layer_shift,
        spatial,
        spatial_shift,
        mixer_down,
    )
    result = half_again(second, gain_after, proj_gate, proj_lift, proj_down)
    return result


def solution(mesh):
    placed = (
        P(("rep", "fs", "tp"), None),
        P(),
        P(),
        P("fs", "tp"),
        P("fs", "tp"),
        P("tp", "fs"),
        P(),
        P("fs", "tp"),
        P("fs", "tp"),
        P("tp"),
        P("tp"),
        P("tp", None, None),
        P("tp", None),
        P("tp", "fs"),
    )
    return jax.shard_map(
        body, mesh=mesh, in_specs=placed, out_specs=P(("rep", "fs", "tp"), None), check_vma=False
    )
```

profile of v0, /device:TPU:0, one launch (start us, length us, event | category | flops | bytes accessed | tf_op | source)
XLA Modules:
  0.0 575.2 jit_solution(15976335767558670113)
XLA Ops:
  6.5 0.0 all-gather.10.cloned.1.call-start
  6.5 0.7 all-gather.10.cloned.1.call-update
  7.3 0.0 all-gather.12.cloned.1.call-start
  7.3 0.7 all-gather.12.cloned.1.call-update
  8.0 0.0 copy-start.10
  8.0 0.0 all-gather.14.cloned.1.call-start
  8.1 0.7 all-gather.14.cloned.1.call-update
  8.8 0.0 all-gather.16.cloned.1.call-start
  8.8 0.5 all-gather.16.cloned.1.call-update
  9.3 0.0 reduce-scatter.4.cloned.1.call-start
  9.4 24.8 %all-gather.10.cloned.1.call-done = bf16[512,2048]{1,0:T(8,128)(2,1)} async-done(((bf16[128,2048]{1,0:T(8,128)(2,1)}), bf16[512,2048]{1,0:T(8,128)(2,1)}) %all-gather.10.cloned.1.call-update) | async-done | bytes 2097168 | tf_op jit(solution)/shard_map/all_gather | solution.py:22
  34.2 2.2 fusion
  36.4 71.5 %all-gather.12.cloned.1.call-done = bf16[2048,896]{1,0:T(8,128)(2,1)} async-done(((bf16[512,896]{1,0:T(8,128)(2,1)}), bf16[2048,896]{1,0:T(8,128)(2,1)}) %all-gather.12.cloned.1.call-update) | async-done | bytes 3670032 | tf_op jit(solution)/shard_map/all_gather | solution.py:42
  107.9 0.0 copy-done.10
  107.9 0.0 copy-done.4
  107.9 5.6 fusion.42
  113.5 66.6 %all-gather.14.cloned.1.call-done = bf16[2048,896]{1,0:T(8,128)(2,1)} async-done(((bf16[512,896]{1,0:T(8,128)(2,1)}), bf16[2048,896]{1,0:T(8,128)(2,1)}) %all-gather.14.cloned.1.call-update) | async-done | bytes 3670032 | tf_op jit(solution)/shard_map/all_gather | solution.py:43
  180.2 72.1 %all-gather.16.cloned.1.call-done = bf16[896,2048]{1,0:T(8,128)(2,1)} async-done(((bf16[896,512]{1,0:T(8,128)(2,1)}), bf16[896,2048]{1,0:T(8,128)(2,1)}) %all-gather.16.cloned.1.call-update) | async-done | bytes 3670032 | tf_op jit(solution)/shard_map/all_gather | solution.py:49
  252.3 9.7 %convolution_convert_fusion.1 = bf16[512,2048]{1,0:T(8,128)(2,1)} fusion(bf16[896,2048]{1,0:T(8,128)(2,1)} %all-gather.16.cloned.1.call-done, f32[512,896]{1,0:T(8,128)} %fusion.42, bf16[2048,896]{1,0:T(8,128)(2,1)} %all-gather.14.cloned.1.call-done, bf16[512,2048]{1,0:T(8,128)(2,1)S(1)} %copy-done.4, f32[2048]{0:T(1024)S(1)} %copy-done.10, ...), kind=kOutput, calls=%fused_computation.16 | convolution fusion | flops 3766091776 | bytes 13379584 | tf_op jit(solution)/shard_map/dot_general | solution.py:47
  262.0 0.0 reduce-scatter.4.cloned.1.call-update
  262.0 0.0 all-gather.18.cloned.1.call-start
  262.0 29.9 %reduce-scatter.4.cloned.1.call-done = bf16[128,2048]{1,0:T(8,128)(2,1)} async-done(((bf16[512,2048]{1,0:T(8,128)(2,1)}), bf16[128,2048]{1,0:T(8,128)(2,1)}) %reduce-scatter.4.cloned.1.call-update) | async-done | bytes 524304 | tf_op jit(solution)/shard_map/reduce_scatter | solution.py:52
  291.9 0.0 copy-done.2
  291.9 2.0 add_convert_fusion.3
  293.9 0.0 all-gather.18.cloned.1.call-update
  293.9 0.0 all-gather.22.cloned.1.call-start
  294.0 0.7 all-gather.22.cloned.1.call-update
  294.7 0.0 all-gather.20.cloned.1.call-start
  294.7 0.7 all-gather.20.cloned.1.call-update
  295.4 0.0 all-gather.24.cloned.1.call-start
  295.5 0.7 all-gather.24.cloned.1.call-update
  296.2 0.0 reduce-scatter.6.cloned.1.call-start
  296.2 20.4 %all-gather.18.cloned.1.call-done = bf16[512,2048]{1,0:T(8,128)(2,1)} async-done(((bf16[128,2048]{1,0:T(8,128)(2,1)}), bf16[512,2048]{1,0:T(8,128)(2,1)}) %all-gather.18.cloned.1.call-update) | async-done | bytes 2097168 | tf_op jit(solution)/shard_map/all_gather | solution.py:69
  316.6 2.2 fusion.3
  318.9 0.0 copy-start.7
  318.9 0.0 copy-start.8
  318.9 45.0 %all-gather.22.cloned.1.call-done = bf16[2048,512]{1,0:T(8,128)(2,1)} async-done(((bf16[512,512]{1,0:T(8,128)(2,1)}), bf16[2048,512]{1,0:T(8,128)(2,1)}) %all-gather.22.cloned.1.call-update) | async-done | bytes 2097168 | tf_op jit(solution)/shard_map/all_gather | solution.py:76
  363.9 0.0 copy-done.11
  363.9 0.0 copy-done.3
  363.9 4.1 fusion.60
  368.0 6.5 %all-reduce = (f32[512]{0:T(512)S(1)}, f32[512]{0:T(512)S(1)}) all-reduce(f32[512]{0:T(512)S(1)} %get-tuple-element.6, f32[512]{0:T(512)S(1)} %get-tuple-element.5), channel_id=1, replica_groups=mesh['rep'=2,'fs'=4,'tp'=4] {'tp'}, use_global_device_ids=true, to_apply=%region_6.7 | all-reduce | flops 1024 | bytes 8192 | tf_op jit(solution)/shard_map/psum | solution.py:80
  374.6 0.0 copy-done.7
  374.6 1.5 add_convert_fusion.2
  376.0 0.9 reshape.47
  377.0 1.4 fusion.9
  378.4 1.3 copy.21
  379.7 30.2 %all-gather.20.cloned.1.call-done = bf16[2048,512]{1,0:T(8,128)(2,1)} async-done(((bf16[512,512]{1,0:T(8,128)(2,1)}), bf16[2048,512]{1,0:T(8,128)(2,1)}) %all-gather.20.cloned.1.call-update) | async-done | bytes 2097168 | tf_op jit(solution)/shard_map/all_gather | solution.py:75
  409.9 46.1 %all-gather.24.cloned.1.call-done = bf16[512,2048]{1,0:T(8,128)(2,1)} async-done(((bf16[512,512]{1,0:T(8,128)(2,1)}), bf16[512,2048]{1,0:T(8,128)(2,1)}) %all-gather.24.cloned.1.call-update) | async-done | bytes 2097168 | tf_op jit(solution)/shard_map/all_gather | solution.py:98
  456.0 6.5 %convolution_convert_fusion.2 = bf16[512,2048]{1,0:T(8,128)(2,1)} fusion(bf16[512,2048]{1,0:T(8,128)(2,1)} %all-gather.24.cloned.1.call-done, f32[64,8,4,128]{3,2,1,0:T(4,128)} %bitcast.25, bf16[2048,512]{1,0:T(8,128)(2,1)} %all-gather.20.cloned.1.call-done, bf16[512,2048]{1,0:T(8,128)(2,1)S(1)} %copy-done.3, f32[2048]{0:T(1024)S(1)} %copy-done.11, ...), kind=kOutput, calls=%fused_computation.17 | convolution fusion | flops 2155347968 | bytes 9447424 | tf_op jit(solution)/shard_map/dot_general | solution.py:96
  462.5 0.0 reduce-scatter.6.cloned.1.call-update
  462.5 0.0 copy-start.12
  462.5 0.0 all-gather.26.cloned.1.call-start
  462.6 30.1 %reduce-scatter.6.cloned.1.call-done = bf16[128,2048]{1,0:T(8,128)(2,1)} async-done(((bf16[512,2048]{1,0:T(8,128)(2,1)}), bf16[128,2048]{1,0:T(8,128)(2,1)}) %reduce-scatter.6.cloned.1.call-update) | async-done | bytes 524304 | tf_op jit(solution)/shard_map/reduce_scatter | solution.py:101
  492.7 2.0 add_convert_fusion.1
  494.6 0.0 all-gather.26.cloned.1.call-update
  494.6 0.2 reduce-scatter.8.cloned.1.call-start
  494.9 22.5 %all-gather.26.cloned.1.call-done = bf16[512,2048]{1,0:T(8,128)(2,1)} async-done(((bf16[128,2048]{1,0:T(8,128)(2,1)}), bf16[512,2048]{1,0:T(8,128)(2,1)}) %all-gather.26.cloned.1.call-update) | async-done | bytes 2097168 | tf_op jit(solution)/shard_map/all_gather | solution.py:22
  517.4 2.2 fusion.6
  519.6 0.0 copy-done.12
  519.6 5.7 fusion.28
  525.3 9.7 %convolution_convert_fusion = bf16[512,2048]{1,0:T(8,128)(2,1)} fusion(bf16[896,2048]{1,0:T(8,128)(2,1)} %all-gather.16.cloned.1.call-done, f32[512,896]{1,0:T(8,128)} %fusion.28, bf16[2048,896]{1,0:T(8,128)(2,1)} %all-gather.14.cloned.1.call-done, bf16[512,2048]{1,0:T(8,128)(2,1)S(1)} %copy-done.5, f32[2048]{0:T(1024)S(1)} %copy-done.12, ...), kind=kOutput, calls=%fused_computation.15 | convolution fusion | flops 3766091776 | bytes 13379584 | tf_op jit(solution)/shard_map/dot_general | solution.py:47
  535.0 0.0 reduce-scatter.8.cloned.1.call-update
  535.0 31.3 %reduce-scatter.8.cloned.1.call-done = bf16[128,2048]{1,0:T(8,128)(2,1)} async-done(((bf16[512,2048]{1,0:T(8,128)(2,1)}), bf16[128,2048]{1,0:T(8,128)(2,1)}) %reduce-scatter.8.cloned.1.call-update) | async-done | bytes 524304 | tf_op jit(solution)/shard_map/reduce_scatter | solution.py:52
  566.4 2.0 add_convert_fusion
  (20 shorter events, 0.1 us)
Async XLA Ops:
  6.5 27.7 %all-gather.10.cloned.1.call-start = ((), (), s32[]{:S(2)}) async-start(), calls=%async_computation.3 | async-start | bytes 2621440 | tf_op jit(solution)/shard_map/all_gather | solution.py:22
  7.3 100.6 %all-gather.12.cloned.1.call-start = ((), (), s32[]{:S(2)}) async-start(), calls=%async_computation.4 | async-start | bytes 4587520 | tf_op jit(solution)/shard_map/all_gather | solution.py:42
  8.0 99.9 %copy-start.10 = (f32[2048]{0:T(1024)S(1)}, f32[2048]{0:T(1024)}, u32[]{:S(2)}) copy-start(f32[2048]{0:T(1024)} %param.15) | copy-start | bytes 24580
  8.0 172.2 %all-gather.14.cloned.1.call-start = ((), (), s32[]{:S(2)}) async-start(), calls=%async_computation.5 | async-start | bytes 4587520 | tf_op jit(solution)/shard_map/all_gather | solution.py:43
  8.8 243.5 %all-gather.16.cloned.1.call-start = ((), (), s32[]{:S(2)}) async-start(), calls=%async_computation.6 | async-start | bytes 4587520 | tf_op jit(solution)/shard_map/all_gather | solution.py:49
  9.3 282.6 %reduce-scatter.4.cloned.1.call-start = ((), (), s32[]{:S(2)}) async-start(), calls=%async_computation.7 | async-start | bytes 2621440 | tf_op jit(solution)/shard_map/reduce_scatter | solution.py:52
  34.2 73.7 %copy-start.4 = (bf16[512,2048]{1,0:T(8,128)(2,1)S(1)}, bf16[512,2048]{1,0:T(8,128)(2,1)}, u32[]{:S(2)}) copy-start(bf16[512,2048]{1,0:T(8,128)(2,1)} %all-gather.10.cloned.1.call-done) | copy-start | bytes 6291460
  262.0 29.9 %copy-start.2 = (bf16[128,2048]{1,0:T(8,128)(2,1)S(1)}, bf16[128,2048]{1,0:T(8,128)(2,1)}, u32[]{:S(2)}) copy-start(bf16[128,2048]{1,0:T(8,128)(2,1)} %param.14) | copy-start | bytes 1572868
  262.0 54.6 %all-gather.18.cloned.1.call-start = ((), (), s32[]{:S(2)}) async-start(), calls=%async_computation.8 | async-start | bytes 2621440 | tf_op jit(solution)/shard_map/all_gather | solution.py:69
  293.9 70.0 %copy-start.11 = (f32[2048]{0:T(1024)S(1)}, f32[2048]{0:T(1024)}, u32[]{:S(2)}) copy-start(f32[2048]{0:T(1024)} %param.20) | copy-start | bytes 24580
  293.9 70.0 %all-gather.22.cloned.1.call-start = ((), (), s32[]{:S(2)}) async-start(), calls=%async_computation.10 | async-start | bytes 2621440 | tf_op jit(solution)/shard_map/all_gather | solution.py:76
  294.7 115.3 %all-gather.20.cloned.1.call-start = ((), (), s32[]{:S(2)}) async-start(), calls=%async_computation.9 | async-start | bytes 2621440 | tf_op jit(solution)/shard_map/all_gather | solution.py:75
  295.4 160.6 %all-gather.24.cloned.1.call-start = ((), (), s32[]{:S(2)}) async-start(), calls=%async_computation.11 | async-start | bytes 2621440 | tf_op jit(solution)/shard_map/all_gather | solution.py:98
  296.2 196.5 %reduce-scatter.6.cloned.1.call-start = ((), (), s32[]{:S(2)}) async-start(), calls=%async_computation.12 | async-start | bytes 2621440 | tf_op jit(solution)/shard_map/reduce_scatter | solution.py:101
  316.6 47.3 %copy-start.3 = (bf16[512,2048]{1,0:T(8,128)(2,1)S(1)}, bf16[512,2048]{1,0:T(8,128)(2,1)}, u32[]{:S(2)}) copy-start(bf16[512,2048]{1,0:T(8,128)(2,1)} %all-gather.18.cloned.1.call-done) | copy-start | bytes 6291460
  318.9 55.7 %copy-start.7 = (f32[512]{0:T(512)S(1)}, f32[512]{0:T(512)}, u32[]{:S(2)}) copy-start(f32[512]{0:T(512)} %param.24) | copy-start | bytes 6148
  318.9 55.7 %copy-start.8 = (f32[512]{0:T(512)S(1)}, f32[512]{0:T(512)}, u32[]{:S(2)}) copy-start(f32[512]{0:T(512)} %param.23) | copy-start | bytes 6148
  368.0 8.9 %copy-start.6 = (bf16[4,128,128]{2,1,0:T(8,128)(2,1)S(1)}, bf16[4,128,128]{2,1,0:T(8,128)(2,1)}, u32[]{:S(2)}) copy-start(bf16[4,128,128]{2,1,0:T(8,128)(2,1)} %param.25) | copy-start | bytes 393220
  368.0 8.9 %copy-start.9 = (f32[4,128]{1,0:T(4,128)S(1)}, f32[4,128]{1,0:T(4,128)}, u32[]{:S(2)}) copy-start(f32[4,128]{1,0:T(4,128)} %param.26) | copy-start | bytes 6148
  462.5 30.2 %copy-start = (bf16[128,2048]{1,0:T(8,128)(2,1)S(1)}, bf16[128,2048]{1,0:T(8,128)(2,1)}, u32[]{:S(2)}) copy-start(bf16[128,2048]{1,0:T(8,128)(2,1)} %add_convert_fusion.3) | copy-start | bytes 1572868
  462.5 57.1 %copy-start.12 = (f32[2048]{0:T(1024)S(1)}, f32[2048]{0:T(1024)}, u32[]{:S(2)}) copy-start(f32[2048]{0:T(1024)} %param.16) | copy-start | bytes 24580
  462.5 54.8 %all-gather.26.cloned.1.call-start = ((), (), s32[]{:S(2)}) async-start(), calls=%async_computation.13 | async-start | bytes 2621440 | tf_op jit(solution)/shard_map/all_gather | solution.py:22
  494.6 71.7 %reduce-scatter.8.cloned.1.call-start = ((), (), s32[]{:S(2)}) async-start(), calls=%async_computation.14 | async-start | bytes 2621440 | tf_op jit(solution)/shard_map/reduce_scatter | solution.py:52
  517.4 2.2 copy-start.5
  535.0 31.4 %copy-start.1 = (bf16[128,2048]{1,0:T(8,128)(2,1)S(1)}, bf16[128,2048]{1,0:T(8,128)(2,1)}, u32[]{:S(2)}) copy-start(bf16[128,2048]{1,0:T(8,128)(2,1)} %add_convert_fusion.1) | copy-start | bytes 1572868
Sparse Core Ops, SparseCore 0:
  8.9 25.2 all-gather.9
  35.8 72.0 all-gather.11
  109.5 70.6 all-gather.13
  181.6 70.6 all-gather.15
  262.1 29.7 reduce-scatter.3
  294.1 22.5 all-gather.17
  318.2 45.6 all-gather.21
  365.5 44.4 all-gather.19
  411.5 44.4 all-gather.23
  462.6 29.9 reduce-scatter.5
  494.8 22.5 all-gather.25
  535.1 31.1 reduce-scatter.7
where the time goes:
time: 576 us; the launch traced here: 575 us
  waiting for transfers between devices  495 us (86%)
  matrix products  42.7 us (7%)
  other arithmetic  14.1 us (2%)
  between operations  13.7 us (2%)
  blocking collectives  6.51 us (1%)
    all_gather x1, waiting for transfers between devices, half_again(): lax.all_gather(proj_down, 'fs', axis=1, tiled=True)  72.1 us
    all_gather x1, waiting for transfers between devices, half_again(): lax.all_gather(proj_gate, 'fs', axis=0, tiled=True)  71.5 us
    all_gather x1, waiting for transfers between devices, half_again(): lax.all_gather(proj_lift, 'fs', axis=0, tiled=True)  66.6 us
    reduce_scatter x2, waiting for transfers between devices, half_again(): lax.psum_scatter(partial_value.astype(jnp.bfloat16), 'tp', scatter_dimens...  61.2 us
    all_gather x2, waiting for transfers between devices, gathered_norm(): gathered = lax.all_gather(stream_rows, 'tp', axis=0, tiled=True)  47.3 us
    all_gather x1, waiting for transfers between devices, token_mixer(): lax.all_gather(mixer_down, 'fs', axis=1, tiled=True)  46.1 us
    all_gather x1, waiting for transfers between devices, token_mixer(): lax.all_gather(mixer_v, 'fs', axis=0, tiled=True)  45 us
    all_gather x1, waiting for transfers between devices, token_mixer(): lax.all_gather(mixer_u, 'fs', axis=0, tiled=True)  30.2 us
  transfers between devices with their start and end apart: 12, of which 12 were waited for; matrix products, arithmetic and copies ran while one was open for 3% of the time, Pallas kernels for 0%

commit v1 on v0

v1 whole, which is shorter than its diff:
```python
import functools

import jax
import jax.numpy as jnp
from jax import lax
from jax.experimental import pallas as pl
from jax.experimental.pallas import tpu as pltpu
from jax.sharding import PartitionSpec as P

SPAN = 128

norm_epsilon = 1e-06
layer_epsilon = 1e-05

MESH = pl.DeviceIdType.MESH
GATE, LIFT, DOWN, MIX_U, MIX_V, MIX_DOWN = range(6)


def norm_rows(widened, scale_gain):
    factor = lax.rsqrt(jnp.mean(widened * widened, axis=1, keepdims=True) + norm_epsilon)
    return (widened * factor * scale_gain).astype(jnp.bfloat16)


def layer_kernel(
    n_rep,
    n_fs,
    n_tp,
    stream,
    gain_before,
    gain_after,
    mixer_gain,
    layer_gain,
    layer_shift,
    spatial,
    spatial_shift,
    proj_gate,
    proj_lift,
    proj_down,
    mixer_u,
    mixer_v,
    mixer_down,
    out,
    gate_all,
    lift_all,
    down_all,
    u_all,
    v_all,
    mix_down_all,
    rows_all,
    to_sibling,
    from_sibling,
    to_chip,
    from_chip,
    partial_all,
    gate_vals,
    hidden,
    u_vals,
    lifted,
    gated,
    mom_own,
    mom_in,
    square,
    resid,
    local_sem,
    z_send,
    z_send_left,
    z_recv,
    y_send,
    y_recv,
    ag_sem,
    agf_sem,
    sib_sem,
    chip_sem,
    mom_sem,
):
    rep, fs, tp = lax.axis_index("rep"), lax.axis_index("fs"), lax.axis_index("tp")
    chip, core = tp // 2, lax.rem(tp, 2)
    n_chip = n_tp // 2
    block, width = stream.shape
    pair = 2 * block
    shards = (proj_gate, proj_lift, proj_down, mixer_u, mixer_v, mixer_down)
    full = (gate_all, lift_all, down_all, u_all, v_all, mix_down_all)
    mine = pl.ds(pl.multiple_of(core * block, block), block)
    theirs = pl.ds(pl.multiple_of((1 - core) * block, block), block)
    sibling = chip * 2 + (1 - core)

    def at(r, f, t):
        return (r, f, t)

    barrier = pltpu.get_barrier_semaphore()

    @pl.when(fs > 0)
    def _():
        pl.semaphore_signal(barrier, inc=1, device_id=at(rep, fs - 1, tp), device_id_type=MESH)

    @pl.when(fs < n_fs - 1)
    def _():
        pl.semaphore_signal(barrier, inc=1, device_id=at(rep, fs + 1, tp), device_id_type=MESH)

    for k in range(1, n_rep):
        pl.semaphore_signal(
            barrier, inc=1, device_id=at(lax.rem(rep + k, n_rep), fs, tp), device_id_type=MESH
        )
    for k in range(1, n_tp):
        pl.semaphore_signal(
            barrier, inc=1, device_id=at(rep, fs, lax.rem(tp + k, n_tp)), device_id_type=MESH
        )

    locals_ = [
        pltpu.make_async_copy(shards[w], full[w].at[fs], local_sem.at[w]) for w in range(6)
    ]
    for copy in locals_:
        copy.start()

    line_peers = jnp.minimum(fs, 1) + jnp.minimum(n_fs - 1 - fs, 1)
    pl.semaphore_wait(barrier, n_rep - 1 + n_tp - 1 + line_peers)

    def piece(w, owner, part):
        rows = full[w].shape[1] // n_rep
        return full[w].at[owner, pl.ds(pl.multiple_of(part * rows, rows), rows)]

    def z_copy(w, owner, step):
        ref = piece(w, owner, rep)
        sem = z_send.at[w, owner] if step > 0 else z_send_left.at[w, owner]
        return pltpu.make_async_remote_copy(
            src_ref=ref, dst_ref=ref, send_sem=sem, recv_sem=z_recv.at[w, owner],
            device_id=at(rep, fs + step, tp), device_id_type=MESH,
        )

    def y_copy(w, owner, k):
        ref = piece(w, owner, rep)
        return pltpu.make_async_remote_copy(
            src_ref=ref, dst_ref=ref, send_sem=y_send.at[w, k - 1, owner],
            recv_sem=y_recv.at[w, k - 1, owner],
            device_id=at(lax.rem(rep + k, n_rep), fs, tp), device_id_type=MESH,
        )

    def own(w):
        locals_[w].wait()

        @pl.when(fs < n_fs - 1)
        def _():
            z_copy(w, fs, 1).start()

        @pl.when(fs > 0)
        def _():
            z_copy(w, fs, -1).start()

    def pump(w):
        def hop(h, carry):
            @pl.when(fs >= h)
            def _():
                z_copy(w, fs - h, 1).wait_recv()
                for k in range(1, n_rep):
                    y_copy(w, fs - h, k).start()

                @pl.when(fs < n_fs - 1)
                def _():
                    z_copy(w, fs - h, 1).start()

            @pl.when(fs + h < n_fs)
            def _():
                z_copy(w, fs + h, -1).wait_recv()
                for k in range(1, n_rep):
                    y_copy(w, fs + h, k).start()

                @pl.when(fs > 0)
                def _():
                    z_copy(w, fs + h, -1).start()

            return carry

        lax.fori_loop(1, n_fs, hop, 0)

    def arrived(w):
        def one(h, carry):
            owner = lax.rem(fs + h, n_fs)
            for k in range(1, n_rep):
                source = lax.rem(rep + n_rep - k, n_rep)
                ref = piece(w, owner, source)
                pltpu.make_async_remote_copy(
                    src_ref=ref, dst_ref=ref, send_sem=y_send.at[w, k - 1, owner],
                    recv_sem=y_recv.at[w, k - 1, owner],
                    device_id=at(source, fs, tp), device_id_type=MESH,
                ).wait_recv()
            return carry

        lax.fori_loop(1, n_fs, one, 0)

    def sends_done():
        def one(owner, carry):
            for w in range(6):
                @pl.when((owner <= fs) & (fs < n_fs - 1))
                def _():
                    z_copy(w, owner, 1).wait_send()

                @pl.when((owner >= fs) & (fs > 0))
                def _():
                    z_copy(w, owner, -1).wait_send()

                @pl.when(owner != fs)
                def _():
                    for k in range(1, n_rep):
                        y_copy(w, owner, k).wait_send()

            return carry

        lax.fori_loop(0, n_fs, one, 0)

    def other_chip(k):
        return lax.rem(chip + k, n_chip)

    def source_chip(k):
        return lax.rem(chip + n_chip - k, n_chip)

    def tp_copy(src, dst, send, recv, target):
        return pltpu.make_async_remote_copy(
            src_ref=src, dst_ref=dst, send_sem=send, recv_sem=recv,
            device_id=at(rep, fs, target), device_id_type=MESH,
        )

    def gather_copy(phase, k):
        ref = rows_all.at[phase, chip, mine]
        target = other_chip(k) * 2 + core
        return tp_copy(ref, ref, ag_sem.at[0, phase, k], ag_sem.at[1, phase, k], target)

    def pass_copy(phase, k):
        ref = rows_all.at[phase, source_chip(k), mine]
        return tp_copy(ref, ref, agf_sem.at[0, phase, k], agf_sem.at[1, phase, k], sibling)

    def gather_start(phase, normed):
        rows_all[phase, chip, mine] = normed
        for k in range(1, n_chip):
            gather_copy(phase, k).start()
        pass_copy(phase, 0).start()

    def gather_pass(phase):
        for k in range(1, n_chip):
            gather_copy(phase, k).wait_recv()
            pass_copy(phase, k).start()

    def gather_end(phase):
        for k in range(1, n_chip):
            gather_copy(phase, k).wait_send()
        for k in range(n_chip):
            pass_copy(phase, k).wait_send()

    def each_pair(compute):
        def one(p, carry):
            compute(p)
            return carry

        lax.fori_loop(0, n_chip, one, 0)

    def sib_copy(phase, p):
        return tp_copy(
            to_sibling.at[phase, p], from_sibling.at[phase, p],
            sib_sem.at[0, phase, p], sib_sem.at[1, phase, p], sibling,
        )

    def chip_copy(phase, k):
        return tp_copy(
            to_chip.at[phase, k - 1], from_chip.at[phase, k - 1],
            chip_sem.at[0, phase, k], chip_sem.at[1, phase, k], other_chip(k) * 2 + core,
        )

    def reduce(phase, left, w):
        cols = full[w].shape[2]

        def product(p):
            def one(f, carry):
                partial_all[f] = jnp.dot(left[p], full[w][f], preferred_element_type=jnp.float32)
                return carry

            lax.fori_loop(0, n_fs, one, 0)
            for f in range(n_fs):
                to_sibling[phase, p, :, f * cols : (f + 1) * cols] = partial_all[f, theirs].astype(
                    jnp.bfloat16
                )
            sib_copy(phase, p).start()

        def joined(p):
            sib_copy(phase, p).wait_recv()
            held = jnp.concatenate([partial_all[f, mine] for f in range(n_fs)], axis=1)
            return held + from_sibling[phase, p].astype(jnp.float32)

        def away(k, carry):
            p = other_chip(k)
            product(p)
            to_chip[phase, k - 1] = joined(p).astype(jnp.bfloat16)
            chip_copy(phase, k).start()
            return carry

        lax.fori_loop(1, n_chip, away, 0)
        product(chip)
        total = joined(chip)
        for k in range(1, n_chip):
            chip_copy(phase, k).wait_recv()
            total = total + from_chip[phase, k - 1].astype(jnp.float32)
        for k in range(1, n_chip):
            chip_copy(phase, k).wait_send()
        for p in range(n_chip):
            sib_copy(phase, p).wait_send()
        return total

    def project(phase, p, w):
        rows = full[w].shape[1]
        total = None
        for f in range(n_fs):
            term = jnp.dot(
                rows_all[phase, p, :, f * rows : (f + 1) * rows], full[w][f],
                preferred_element_type=jnp.float32,
            )
            total = term if total is None else total + term
        return total

    def gate_pair(phase):
        def compute(p):
            gate_vals[p] = project(phase, p, GATE)

        return compute

    def lift_pair(phase):
        def compute(p):
            hidden[p] = (jax.nn.silu(gate_vals[p]) * project(phase, p, LIFT)).astype(jnp.bfloat16)

        return compute

    gather_start(0, norm_rows(stream[...].astype(jnp.float32), gain_before[...]))
    own(GATE)
    own(LIFT)
    pass_copy(0, 0).wait_recv()
    pump(GATE)
    gather_pass(0)
    for k in range(1, n_chip):
        pass_copy(0, k).wait_recv()
    arrived(GATE)
    each_pair(gate_pair(0))
    own(DOWN)
    pump(LIFT)
    arrived(LIFT)
    each_pair(lift_pair(0))
    own(MIX_U)
    pump(DOWN)
    own(MIX_V)
    own(MIX_DOWN)
    arrived(DOWN)
    total = reduce(0, hidden, DOWN)
    first = (stream[...].astype(jnp.float32) + 0.5 * total).astype(jnp.bfloat16)
    resid[...] = first
    gather_end(0)

    gather_start(1, norm_rows(first.astype(jnp.float32), mixer_gain[...]))
    pump(MIX_U)
    pass_copy(1, 0).wait_recv()
    gather_pass(1)
    for k in range(1, n_chip):
        pass_copy(1, k).wait_recv()
    arrived(MIX_U)

    def u_pair(p):
        u_vals[p] = jax.nn.gelu(project(1, p, MIX_U))

    each_pair(u_pair)
    pump(MIX_V)
    arrived(MIX_V)

    def v_pair(p):
        values = jax.nn.gelu(project(1, p, MIX_V))
        lifted[p] = values
        sums = jnp.sum(values, axis=1, keepdims=True)
        squares = jnp.sum(values * values, axis=1, keepdims=True)
        lane = lax.broadcasted_iota(jnp.int32, (pair, 128), 1)
        both = jnp.where(lane == 0, sums, jnp.where(lane == 1, squares, 0.0))
        mom_own[p] = both.T[:8]

    each_pair(v_pair)

    def mom_copy(k):
        return tp_copy(
            mom_own, mom_in.at[k - 1], mom_sem.at[0, k], mom_sem.at[1, k], lax.rem(tp + k, n_tp)
        )

    for k in range(1, n_tp):
        mom_copy(k).start()
    pump(MIX_DOWN)
    square[...] = jnp.zeros_like(square)
    groups = spatial.shape[0]
    square[0:groups, :] = spatial_shift[...]
    shift_columns = square[...].T
    for k in range(1, n_tp):
        mom_copy(k).wait_recv()
    channels = lifted.shape[2]
    group_dim = channels // groups
    all_channels = channels * n_tp

    def mix_pair(p):
        moments = mom_own[p]
        for k in range(1, n_tp):
            moments = moments + mom_in[k - 1, p]
        moments = moments * (1.0 / all_channels)
        columns = jnp.concatenate([moments, jnp.zeros((120, pair), jnp.float32)], axis=0).T
        centre = columns[:, 0:1]
        spread = columns[:, 1:2] - centre * centre
        normed_v = (
            (lifted[p] - centre) * lax.rsqrt(spread + layer_epsilon) * layer_gain[...]
            + layer_shift[...]
        ).astype(jnp.bfloat16)
        row = lax.broadcasted_iota(jnp.int32, (SPAN, SPAN), 0)
        col = lax.broadcasted_iota(jnp.int32, (SPAN, SPAN), 1)
        for g in range(groups):
            masked = jnp.where(row >= col, spatial[g].astype(jnp.float32), 0.0).astype(
                jnp.bfloat16
            )
            cut = slice(g * group_dim, (g + 1) * group_dim)
            for b in range(pair // SPAN):
                span = slice(b * SPAN, (b + 1) * SPAN)
                mixed = jnp.dot(masked, normed_v[span, cut], preferred_element_type=jnp.float32)
                mixed = mixed + shift_columns[:, g : g + 1]
                gated[p, span, cut] = (u_vals[p, span, cut] * mixed).astype(jnp.bfloat16)

    each_pair(mix_pair)
    for k in range(1, n_tp):
        mom_copy(k).wait_send()
    arrived(MIX_DOWN)
    total = reduce(1, gated, MIX_DOWN)
    second = (resid[...].astype(jnp.float32) + total).astype(jnp.bfloat16)
    resid[...] = second
    gather_end(1)

    gather_start(2, norm_rows(second.astype(jnp.float32), gain_after[...]))
    pass_copy(2, 0).wait_recv()
    gate_pair(2)(chip)
    lift_pair(2)(chip)
    gather_pass(2)
    for k in range(1, n_chip):
        pass_copy(2, k).wait_recv()

    def last_pair(k, carry):
        gate_pair(2)(other_chip(k))
        lift_pair(2)(other_chip(k))
        return carry

    lax.fori_loop(1, n_chip, last_pair, 0)
    total = reduce(2, hidden, DOWN)
    out[...] = (resid[...].astype(jnp.float32) + 0.5 * total).astype(jnp.bfloat16)
    gather_end(2)
    sends_done()


def body(
    n_rep,
    n_fs,
    n_tp,
    stream,
    gain_before,
    gain_after,
    proj_gate,
    proj_lift,
    proj_down,
    mixer_gain,
    mixer_u,
    mixer_v,
    layer_gain,
    layer_shift,
    spatial,
    spatial_shift,
    mixer_down,
):
    block, width = stream.shape
    n_chip = n_tp // 2
    pair = 2 * block
    units = proj_gate.shape[1]
    channels = mixer_u.shape[1]
    bf16, f32 = jnp.bfloat16, jnp.float32
    shards = (proj_gate, proj_lift, proj_down, mixer_u, mixer_v, mixer_down)
    vmem = pl.BlockSpec(memory_space=pltpu.VMEM)
    anywhere = pl.BlockSpec(memory_space=pl.ANY)
    dma = pltpu.SemaphoreType.DMA
    spread_reps = max(n_rep - 1, 1)
    spread_chips = max(n_chip - 1, 1)
    return pl.pallas_call(
        functools.partial(layer_kernel, n_rep, n_fs, n_tp),
        out_shape=jax.ShapeDtypeStruct((block, width), bf16),
        in_specs=[vmem] * 8 + [anywhere] * 6,
        out_specs=vmem,
        scratch_shapes=[pltpu.VMEM((n_fs,) + w.shape, bf16) for w in shards]
        + [
            pltpu.VMEM((3, n_chip, pair, width), bf16),
            pltpu.VMEM((3, n_chip, block, width), bf16),
            pltpu.VMEM((3, n_chip, block, width), bf16),
            pltpu.VMEM((3, spread_chips, block, width), bf16),
            pltpu.VMEM((3, spread_chips, block, width), bf16),
            pltpu.VMEM((n_fs, pair, width // n_fs), f32),
            pltpu.VMEM((n_chip, pair, units), f32),
            pltpu.VMEM((n_chip, pair, units), bf16),
            pltpu.VMEM((n_chip, pair, channels), f32),
            pltpu.VMEM((n_chip, pair, channels), f32),
            pltpu.VMEM((n_chip, pair, channels), bf16),
            pltpu.VMEM((n_chip, 8, pair), f32),
            pltpu.VMEM((max(n_tp - 1, 1), n_chip, 8, pair), f32),
            pltpu.VMEM((128, SPAN), f32),
            pltpu.VMEM((block, width), bf16),
            dma((6,)),
            dma((6, n_fs)),
            dma((6, n_fs)),
            dma((6, n_fs)),
            dma((6, spread_reps, n_fs)),
            dma((6, spread_reps, n_fs)),
            dma((2, 3, n_chip)),
            dma((2, 3, n_chip)),
            dma((2, 3, n_chip)),
            dma((2, 3, n_chip)),
            dma((2, n_tp)),
        ],
        compiler_params=pltpu.CompilerParams(
            collective_id=0, has_side_effects=True, vmem_limit_bytes=60 * 1024 * 1024
        ),
    )(
        stream,
        gain_before.reshape(1, -1),
        gain_after.reshape(1, -1),
        mixer_gain.reshape(1, -1),
        layer_gain.reshape(1, -1),
        layer_shift.reshape(1, -1),
        spatial,
        spatial_shift,
        *shards,
    )


def solution(mesh):
    placed = (
        P(("rep", "fs", "tp"), None),
        P(),
        P(),
        P("fs", "tp"),
        P("fs", "tp"),
        P("tp", "fs"),
        P(),
        P("fs", "tp"),
        P("fs", "tp"),
        P("tp"),
        P("tp"),
        P("tp", None, None),
        P("tp", None),
        P("tp", "fs"),
    )
    sizes = (mesh.shape["rep"], mesh.shape["fs"], mesh.shape["tp"])
    return jax.shard_map(
        functools.partial(body, *sizes),
        mesh=mesh,
        in_specs=placed,
        out_specs=P(("rep", "fs", "tp"), None),
        check_vma=False,
    )
```

time: 576 us -> 252 us (0.44)
  waiting for transfers between devices: 495 us -> 0 us
  Pallas kernels: 0 us -> 250 us
  matrix products: 42.7 us -> 0 us
  other arithmetic: 14.1 us -> 0 us
  between operations: 13.7 us -> 0.01 us
  blocking collectives: 6.51 us -> 0 us
    all_gather x9 -> x0, waiting for transfers between devices: 399 us -> none  [the longest x1 72.1 us: half_again(): lax.all_gather(proj_down, 'fs', axis=1, tiled=True)]
    pallas_call x0 -> x1, Pallas kernels: none -> 250 us  [body(): pl.pallas_call(functools.partial(layer_kernel, n_rep, n_fs, n_tp), out_sh...]
    reduce_scatter x3 -> x0, waiting for transfers between devices: 91.3 us -> none  [the longest x2 61.2 us: half_again(): lax.psum_scatter(partial_value.astype(jnp.bfloat16), 'tp', scatter_dimens...]
    dot_general x7 -> x0, matrix products: 42.7 us -> none  [the longest x2 19.4 us: half_again(): jnp.dot(hidden, lax.all_gather(proj_down, 'fs', axis=1, tiled=True), pref...]
    convert_element_type x4 -> x0, other arithmetic: 7.4 us -> none  [the longest x2 3.99 us: half_again(): return (stream_rows.astype(jnp.float32) + 0.5 * summed).astype(jnp.bfloat16)]
    reduce_sum x3 -> x0, other arithmetic: 6.67 us -> none  [norm_rows(): jnp.mean(widened * widened, axis=1, keepdims=True) + norm_epsilon]
    psum x1 -> x0, blocking collectives: 6.51 us -> none  [token_mixer(): lax.psum((jnp.sum(lifted, axis=1), jnp.sum(lifted * lifted, axis=1)), 'tp')]
  transfers between devices with their start and end apart: 12 -> 0, of which waited for: 12 -> 0; matrix products, arithmetic and copies ran while one was open for 3% -> 0% of each run, Pallas kernels for 0% -> 0%
where the time goes in v1:
time: 252 us
  Pallas kernels  250 us (99%)
    pallas_call x1, Pallas kernels, body(): pl.pallas_call(functools.partial(layer_kernel, n_rep, n_fs, n_tp), out_sh...  250 us

profile of v1, /device:TPU:0, one launch (start us, length us, event | category | flops | bytes accessed | tf_op | source)
XLA Modules:
  0.0 252.0 jit_solution(3499792056823607604)
XLA Ops:
  0.0 250.1 %shard_map.136 = bf16[128,2048]{1,0:T(8,128)(2,1)} custom-call(bf16[128,2048]{1,0:T(8,128)(2,1)} %stream.1, f32[1,2048]{1,0:T(1,128)} %bitcast.5, f32[1,2048]{1,0:T(1,128)} %bitcast.6, f32[1,2048]{1,0:T(1,128)} %bitcast.7, f32[1,512]{1,0:T(1,128)} %bitcast.8, f32[1,512]{1,0:T(1,128)} %bitcast.9, bf16[4,128,128]{2,1,0:T(8,128)(2,1)} %spatial.1, ...), custom_call_target="tpu_custom_call" | custom-call | tf_op jit(solution)/shard_map/pallas_call | solution.py:482
  250.2 1.9 copy.16

commit v2 on v1

--- a/solution.py
+++ b/solution.py
@@ -14,6 +14,8 @@
 
 MESH = pl.DeviceIdType.MESH
 GATE, LIFT, DOWN, MIX_U, MIX_V, MIX_DOWN = range(6)
+CUTS = 2
+AHEAD = 1
 
 
 def norm_rows(widened, scale_gain):
@@ -115,93 +117,109 @@
     line_peers = jnp.minimum(fs, 1) + jnp.minimum(n_fs - 1 - fs, 1)
     pl.semaphore_wait(barrier, n_rep - 1 + n_tp - 1 + line_peers)
 
-    def piece(w, owner, part):
-        rows = full[w].shape[1] // n_rep
-        return full[w].at[owner, pl.ds(pl.multiple_of(part * rows, rows), rows)]
-
-    def z_copy(w, owner, step):
-        ref = piece(w, owner, rep)
-        sem = z_send.at[w, owner] if step > 0 else z_send_left.at[w, owner]
+    items = 6 * CUTS
+
+    def piece(i, owner, part):
+        w, cut = i // CUTS, i % CUTS
+        rows = full[w].shape[1] // (n_rep * CUTS)
+        first_row = pl.multiple_of((part * CUTS + cut) * rows, rows)
+        return full[w].at[owner, pl.ds(first_row, rows)]
+
+    def z_copy(i, owner, step):
+        ref = piece(i, owner, rep)
+        sem = z_send.at[i, owner] if step > 0 else z_send_left.at[i, owner]
         return pltpu.make_async_remote_copy(
-            src_ref=ref, dst_ref=ref, send_sem=sem, recv_sem=z_recv.at[w, owner],
+            src_ref=ref, dst_ref=ref, send_sem=sem, recv_sem=z_recv.at[i, owner],
             device_id=at(rep, fs + step, tp), device_id_type=MESH,
         )
 
-    def y_copy(w, owner, k):
-        ref = piece(w, owner, rep)
+    def y_copy(i, owner, k):
+        ref = piece(i, owner, rep)
         return pltpu.make_async_remote_copy(
-            src_ref=ref, dst_ref=ref, send_sem=y_send.at[w, k - 1, owner],
-            recv_sem=y_recv.at[w, k - 1, owner],
+            src_ref=ref, dst_ref=ref, send_sem=y_send.at[i, k - 1, owner],
+            recv_sem=y_recv.at[i, k - 1, owner],
             device_id=at(lax.rem(rep + k, n_rep), fs, tp), device_id_type=MESH,
         )
 
-    def own(w):
-        locals_[w].wait()
+    def own(i):
+        if i % CUTS == 0:
+            locals_[i // CUTS].wait()
 
         @pl.when(fs < n_fs - 1)
         def _():
-            z_copy(w, fs, 1).start()
+            z_copy(i, fs, 1).start()
 
         @pl.when(fs > 0)
         def _():
-            z_copy(w, fs, -1).start()
-
-    def pump(w):
+            z_copy(i, fs, -1).start()
+
+    def serve(i):
+        if i + AHEAD < items:
+            own(i + AHEAD)
+
         def hop(h, carry):
             @pl.when(fs >= h)
             def _():
-                z_copy(w, fs - h, 1).wait_recv()
-                for k in range(1, n_rep):
-                    y_copy(w, fs - h, k).start()
+                z_copy(i, fs - h, 1).wait_recv()
 
                 @pl.when(fs < n_fs - 1)
                 def _():
-                    z_copy(w, fs - h, 1).start()
+                    z_copy(i, fs - h, 1).start()
+
+                for k in range(1, n_rep):
+                    y_copy(i, fs - h, k).start()
 
             @pl.when(fs + h < n_fs)
             def _():
-                z_copy(w, fs + h, -1).wait_recv()
-                for k in range(1, n_rep):
-                    y_copy(w, fs + h, k).start()
+                z_copy(i, fs + h, -1).wait_recv()
 
                 @pl.when(fs > 0)
                 def _():
-                    z_copy(w, fs + h, -1).start()
+                    z_copy(i, fs + h, -1).start()
+
+                for k in range(1, n_rep):
+                    y_copy(i, fs + h, k).start()
 
             return carry
 
         lax.fori_loop(1, n_fs, hop, 0)
+
+    def pump(w):
+        for cut in range(CUTS):
+            serve(w * CUTS + cut)
 
     def arrived(w):
         def one(h, carry):
             owner = lax.rem(fs + h, n_fs)
-            for k in range(1, n_rep):
-                source = lax.rem(rep + n_rep - k, n_rep)
-                ref = piece(w, owner, source)
-                pltpu.make_async_remote_copy(
-                    src_ref=ref, dst_ref=ref, send_sem=y_send.at[w, k - 1, owner],
-                    recv_sem=y_recv.at[w, k - 1, owner],
-                    device_id=at(source, fs, tp), device_id_type=MESH,
-                ).wait_recv()
+            for cut in range(CUTS):
+                i = w * CUTS + cut
+                for k in range(1, n_rep):
+                    source = lax.rem(rep + n_rep - k, n_rep)
+                    ref = piece(i, owner, source)
+                    pltpu.make_async_remote_copy(
+                        src_ref=ref, dst_ref=ref, send_sem=y_send.at[i, k - 1, owner],
+                        recv_sem=y_recv.at[i, k - 1, owner],
+                        device_id=at(source, fs, tp), device_id_type=MESH,
+                    ).wait_recv()
             return carry
 
         lax.fori_loop(1, n_fs, one, 0)
 
     def sends_done():
         def one(owner, carry):
-            for w in range(6):
+            for i in range(items):
                 @pl.when((owner <= fs) & (fs < n_fs - 1))
                 def _():
-                    z_copy(w, owner, 1).wait_send()
+                    z_copy(i, owner, 1).wait_send()
 
                 @pl.when((owner >= fs) & (fs > 0))
                 def _():
-                    z_copy(w, owner, -1).wait_send()
+                    z_copy(i, owner, -1).wait_send()
 
                 @pl.when(owner != fs)
                 def _():
                     for k in range(1, n_rep):
-                        y_copy(w, owner, k).wait_send()
+                        y_copy(i, owner, k).wait_send()
 
             return carry
 
@@ -264,7 +282,7 @@
             chip_sem.at[0, phase, k], chip_sem.at[1, phase, k], other_chip(k) * 2 + core,
         )
 
-    def reduce(phase, left, w):
+    def reduce(phase, left, w, meanwhile=None):
         cols = full[w].shape[2]
 
         def product(p):
@@ -294,6 +312,8 @@
         lax.fori_loop(1, n_chip, away, 0)
         product(chip)
         total = joined(chip)
+        if meanwhile is not None:
+            meanwhile()
         for k in range(1, n_chip):
             chip_copy(phase, k).wait_recv()
             total = total + from_chip[phase, k - 1].astype(jnp.float32)
@@ -327,8 +347,8 @@
         return compute
 
     gather_start(0, norm_rows(stream[...].astype(jnp.float32), gain_before[...]))
-    own(GATE)
-    own(LIFT)
+    for i in range(AHEAD):
+        own(i)
     pass_copy(0, 0).wait_recv()
     pump(GATE)
     gather_pass(0)
@@ -336,22 +356,18 @@
         pass_copy(0, k).wait_recv()
     arrived(GATE)
     each_pair(gate_pair(0))
-    own(DOWN)
     pump(LIFT)
     arrived(LIFT)
     each_pair(lift_pair(0))
-    own(MIX_U)
     pump(DOWN)
-    own(MIX_V)
-    own(MIX_DOWN)
     arrived(DOWN)
-    total = reduce(0, hidden, DOWN)
+    total = reduce(0, hidden, DOWN, lambda: pump(MIX_U))
     first = (stream[...].astype(jnp.float32) + 0.5 * total).astype(jnp.bfloat16)
     resid[...] = first
     gather_end(0)
 
     gather_start(1, norm_rows(first.astype(jnp.float32), mixer_gain[...]))
-    pump(MIX_U)
+    pump(MIX_V)
     pass_copy(1, 0).wait_recv()
     gather_pass(1)
     for k in range(1, n_chip):
@@ -362,7 +378,6 @@
         u_vals[p] = jax.nn.gelu(project(1, p, MIX_U))
 
     each_pair(u_pair)
-    pump(MIX_V)
     arrived(MIX_V)
 
     def v_pair(p):
@@ -502,11 +517,11 @@
             pltpu.VMEM((128, SPAN), f32),
             pltpu.VMEM((block, width), bf16),
             dma((6,)),
-            dma((6, n_fs)),
-            dma((6, n_fs)),
-            dma((6, n_fs)),
-            dma((6, spread_reps, n_fs)),
-            dma((6, spread_reps, n_fs)),
+            dma((6 * CUTS, n_fs)),
+            dma((6 * CUTS, n_fs)),
+            dma((6 * CUTS, n_fs)),
+            dma((6 * CUTS, spread_reps, n_fs)),
+            dma((6 * CUTS, spread_reps, n_fs)),
             dma((2, 3, n_chip)),
             dma((2, 3, n_chip)),
             dma((2, 3, n_chip)),

time: 252 us -> 229 us (0.909)
  Pallas kernels: 250 us -> 227 us
    pallas_call x1, Pallas kernels: 250 us -> 227 us  [body(): pl.pallas_call(functools.partial(layer_kernel, n_rep, n_fs, n_tp), out_sh...]
where the time goes in v2:
time: 229 us
  Pallas kernels  227 us (99%)
    pallas_call x1, Pallas kernels, body(): pl.pallas_call(functools.partial(layer_kernel, n_rep, n_fs, n_tp), out_sh...  227 us

profile of v2, /device:TPU:0, one launch (start us, length us, event | category | flops | bytes accessed | tf_op | source)
XLA Modules:
  0.0 228.9 jit_solution(1662691711300817000)
XLA Ops:
  0.0 227.0 %shard_map.136 = bf16[128,2048]{1,0:T(8,128)(2,1)} custom-call(bf16[128,2048]{1,0:T(8,128)(2,1)} %stream.1, f32[1,2048]{1,0:T(1,128)} %bitcast.5, f32[1,2048]{1,0:T(1,128)} %bitcast.6, f32[1,2048]{1,0:T(1,128)} %bitcast.7, f32[1,512]{1,0:T(1,128)} %bitcast.8, f32[1,512]{1,0:T(1,128)} %bitcast.9, bf16[4,128,128]{2,1,0:T(8,128)(2,1)} %spatial.1, ...), custom_call_target="tpu_custom_call" | custom-call | tf_op jit(solution)/shard_map/pallas_call | solution.py:497
  227.0 1.9 copy.16
